TPU v7x, 32 devices: a whole 2x2x4 slice. The times are simulated.
32 devices in a mesh: sp: 16 (over z, y, x), tp: 2 (over core).
Axes of the slice: x: 2, y: 2, z: 4, core: 2. Of those that a mesh axis runs over, the one named last changes fastest.
Arguments:
- latent: bfloat16 [4096, 2048], P(('sp', 'tp')), may hold values from -6 to 6
- cond: float32 [2048], replicated, may hold values from -6 to 6
- ctx_mod: float32 [2048], replicated, may hold values from -6 to 6
- context: bfloat16 [512, 2048], P(('sp', 'tp')), may hold values from -6 to 6
- shift_w: float32 [2048, 2048], P('sp', 'tp'), may hold values from -0.125 to 0.125
- scale_w: float32 [2048, 2048], P('sp', 'tp'), may hold values from -0.125 to 0.125
- gate_w: float32 [2048, 2048], P('sp', 'tp'), may hold values from -0.125 to 0.125
- norm_gain: float32 [2048], replicated, may hold values from 0.1 to 1.9
- w_qn: bfloat16 [2048, 2048], P(None, 'tp'), may hold values from -0.125 to 0.125
- w_qr: bfloat16 [2048, 1024], P(None, 'tp'), may hold values from -0.13258252 to 0.13258252
- w_kv_down: bfloat16 [2048, 512], replicated, may hold values from -0.125 to 0.125
- w_rope_key: bfloat16 [2048, 64], replicated, may hold values from -0.13258252 to 0.13258252
- kv_gain: float32 [512], replicated, may hold values from 0.1 to 1.9
- w_key_up: bfloat16 [512, 2048], P(None, 'tp'), may hold values from -0.66015625 to 0.66015625
- w_value_up: bfloat16 [512, 2048], P(None, 'tp'), may hold values from -0.25 to 0.25
- ctx_bias: float32 [16], P('tp'), may hold values from 2 to 3.5
- w_out: bfloat16 [2048, 2048], P('tp'), may hold values from -0.52734375 to 0.52734375
Outputs:
- mixed: bfloat16 [4096, 2048], P(('sp', 'tp'))
All inputs are finite; a program needn't handle non-finite values.
Results may differ from a plain program's by a relative error of at most 0.018.
Values may be sent and summed in bfloat16 or wider, within the bound.
A program may use at most 128 MiB of HBM per device.

v0:
```python
import functools

import jax
import jax.numpy as jnp
from jax import lax
from jax.experimental import pallas as pl
from jax.experimental.pallas import tpu as pltpu
from jax.sharding import PartitionSpec as P

GRID_W = 128
EPS = 1e-06
ROPE_BASE = 10000.0
LANES = 128
LOG2E = 1.4426950408889634
FLAGS = 4
MESH = pl.DeviceIdType.MESH
F32 = jnp.float32
BF16 = jnp.bfloat16


def remote(src, dst, send, recv, device):
    return pltpu.make_async_remote_copy(
        src_ref=src, dst_ref=dst, send_sem=send, recv_sem=recv, device_id=device, device_id_type=MESH
    )


def rotate(values, cosine, sine):
    width = values.shape[-1]
    ahead = pltpu.roll(values, width - 1, 1)
    behind = pltpu.roll(values, 1, 1)
    even = lax.broadcasted_iota(jnp.int32, values.shape, 1) % 2 == 0
    return values * cosine + jnp.where(even, ahead, behind) * sine


def modulation_kernel(
    n_sp, n_tp, rows, ctx_rows,
    pair_ref, shift_w, scale_w, gate_w, x_ref, gain_ref, down_ref, rope_ref, kv_gain_ref, cos_ref, sin_ref,
    h_ref, packed_ref, gate_ref,
    part, landed, reduced, full, mods, send1, recv1, send2, recv2,
):
    me = lax.axis_index("sp")
    mine = lax.axis_index("tp")
    total = n_sp * n_tp
    flat = me * n_tp + mine
    barrier = pltpu.get_barrier_semaphore()

    def greet(i, _):
        other = lax.rem(flat + i, total)
        pl.semaphore_signal(barrier, inc=1, device_id=(other // n_tp, other % n_tp), device_id_type=MESH)
        return 0

    lax.fori_loop(1, total, greet, 0)

    columns = shift_w.shape[1]
    blocks = columns // LANES
    per = -(-6 * blocks // n_sp)
    part[...] = jnp.zeros_like(part)
    pair = pair_ref[...]
    for which, weight in enumerate((shift_w, scale_w, gate_w)):
        product = jnp.dot(pair, weight[...], precision=lax.Precision.HIGHEST, preferred_element_type=F32)
        for row in range(2):
            for block in range(blocks):
                unit = (which * 2 + row) * blocks + block
                part[unit // per, unit % per : unit % per + 1, :] = product[
                    row : row + 1, block * LANES : (block + 1) * LANES
                ]
    pl.semaphore_wait(barrier, total - 1)

    def scatter(i, _):
        other = lax.rem(me + i, n_sp)
        remote(part.at[other], landed.at[me], send1.at[other], recv1.at[me], (other, mine)).start()
        return 0

    lax.fori_loop(1, n_sp, scatter, 0)
    landed[me] = part[me]

    def scattered(i, _):
        other = lax.rem(me + i, n_sp)
        remote(part.at[other], landed.at[other], send1.at[other], recv1.at[other], (other, mine)).wait()
        return 0

    lax.fori_loop(1, n_sp, scattered, 0)
    reduced[...] = jnp.sum(landed[...], axis=0)

    def gather(i, _):
        other = lax.rem(flat + i, total)
        remote(
            reduced, full.at[flat], send2.at[other], recv2.at[flat], (other // n_tp, other % n_tp)
        ).start()
        return 0

    lax.fori_loop(1, total, gather, 0)
    full[flat] = reduced[...]
    x = x_ref[...].astype(F32)
    normed = x * lax.rsqrt(jnp.mean(x * x, axis=-1, keepdims=True) + EPS) * gain_ref[...]

    def gathered(i, _):
        other = lax.rem(flat + i, total)
        remote(
            reduced, full.at[other], send2.at[other], recv2.at[other], (other // n_tp, other % n_tp)
        ).wait()
        return 0

    lax.fori_loop(1, total, gathered, 0)
    for unit in range(6 * blocks):
        row, block = unit // blocks, unit % blocks
        for t in range(n_tp):
            at = t * columns + block * LANES
            mods[row : row + 1, at : at + LANES] = full[(unit // per) * n_tp + t, unit % per : unit % per + 1, :]
    index = lax.broadcasted_iota(jnp.int32, (x.shape[0], 1), 0)
    latent_row = index < rows
    shift = jnp.where(latent_row, mods[0:1, :], mods[1:2, :])
    scale = jnp.where(latent_row, mods[2:3, :], mods[3:4, :])
    h = (normed * (1.0 + scale) + shift).astype(BF16)
    gate_ref[...] = mods[4:5, :]
    h_ref[...] = h[:rows]
    inner = jnp.dot(h, down_ref[...], preferred_element_type=F32)
    inner = inner * lax.rsqrt(jnp.mean(inner * inner, axis=-1, keepdims=True) + EPS)
    rank = inner.shape[1]
    packed_ref[:, :rank] = (inner * kv_gain_ref[...]).astype(BF16)
    rope = rope_ref.shape[1]
    key = jnp.dot(h, rope_ref[...], preferred_element_type=F32)
    key = jnp.concatenate([key, jnp.zeros((key.shape[0], LANES - rope), F32)], axis=1)
    key = rotate(key, cos_ref[...], sin_ref[...])
    lane = lax.broadcasted_iota(jnp.int32, key.shape, 1)
    is_ctx = (index >= rows) & (index < rows + ctx_rows)
    is_pad = index >= rows + ctx_rows
    flag = jnp.where(lane < rope + FLAGS - 1, is_ctx.astype(F32), is_pad.astype(F32))
    key = jnp.where(lane < rope, key, jnp.where(lane < rope + FLAGS, flag, 0.0))
    packed_ref[:, rank:] = key.astype(BF16)


def attention_kernel(
    n_sp, n_tp, heads, nope, rope, factor,
    h_ref, packed_ref, bias_ref, cos_ref, sin_ref, qn_hbm, qr_hbm, ku_hbm, vu_hbm, wo_hbm, latent_ref, gate_ref,
    out_ref,
    qr_ref, qn_ref, ku_ref, vu_ref, wo_ref, load_sem,
    buf, hbuf, q, acc, top, total, att, outbox, inbox, send, recv, send_t, recv_t, send_h, recv_h, send_o, recv_o,
):
    me = lax.axis_index("sp")
    mine = lax.axis_index("tp")
    loads = [
        pltpu.make_async_copy(src, dst, load_sem.at[i])
        for i, (src, dst) in enumerate(
            ((qr_hbm, qr_ref), (qn_hbm, qn_ref), (ku_hbm, ku_ref), (vu_hbm, vu_ref), (wo_hbm, wo_ref))
        )
    ]
    for load in loads:
        load.start()
    nz = n_sp // 4
    z, side = me // 4, me % 4
    y, x = side // 2, side % 2
    odd = mine % 2
    flip_x = y * 2 + (1 - x)
    flip_y = (1 - y) * 2 + x
    side_a = flip_x * (1 - odd) + flip_y * odd
    side_b = flip_y * (1 - odd) + flip_x * odd
    side_ab = 3 - side
    rows = h_ref.shape[0]
    period, width = packed_ref.shape
    rank = ku_ref.shape[0]

    def column_of(step, t):
        return lax.rem(z + step * (1 - 2 * (t % 2)) + 2 * nz, nz)

    def column(step):
        return column_of(step, mine)

    def peer(zz, ss):
        return (zz * 4 + ss, mine)

    ahead, back = peer(column(1), side), peer(column(-1), side)
    to_a, to_b = peer(z, side_a), peer(z, side_b)
    partners = [lax.rem(mine + i, n_tp) for i in range(1, n_tp)]

    barrier = pltpu.get_barrier_semaphore()
    for other in [ahead, back, to_a, to_b] + [(me, t) for t in partners]:
        pl.semaphore_signal(barrier, inc=1, device_id=other, device_id_type=MESH)
    pl.semaphore_wait(barrier, 3 + n_tp)

    def slot(zz, ss, t):
        return buf.at[t, zz, pl.ds(pl.multiple_of(ss * period, period), period)]

    started = []

    def link(step, ss, way, own, device):
        zz = column(step)
        src = packed_ref if own else slot(zz, ss, mine)
        return remote(src, slot(zz, ss, mine), send.at[way, zz, ss], recv.at[zz, ss], device)

    def over(step, ss, own, t):
        zz = column(step)
        src = packed_ref if own else slot(zz, ss, mine)
        return remote(src, slot(zz, ss, mine), send_t.at[t, zz, ss], recv_t.at[mine, zz, ss], (me, t))

    def push(step, ss, way, own, device):
        link(step, ss, way, own, device).start()
        started.append(lambda: link(step, ss, way, own, device))

    def across(step, ss, own=False):
        for t in partners:
            over(step, ss, own, t).start()
            started.append(lambda t=t: over(step, ss, own, t))

    def arrived(zz, ss):
        remote(slot(zz, ss, mine), slot(zz, ss, mine), send.at[0, zz, ss], recv.at[zz, ss], ahead).wait_recv()

    forward = nz // 2
    backward = nz - 1 - forward
    order = [0]
    for j in range(1, forward + 1):
        order.append(-j)
        if j <= backward:
            order.append(j)

    for t in partners:
        copy = remote(h_ref, hbuf.at[mine], send_h.at[t], recv_h.at[mine], (me, t))
        copy.start()
        started.append(lambda copy=copy: copy)

    def event_z(step):
        zz = column(step)
        own = step == 0
        if not own:
            arrived(zz, side)
        if own or (step < 0 and -step < forward):
            push(step, side, 0, own, ahead)
        if own or (step > 0 and step < backward):
            push(step, side, 1, own, back)
        push(step, side, 2, own, to_a)
        push(step, side, 3, own, to_b)
        across(step, side, own)

    def event_a(step):
        zz = column(step)
        arrived(zz, side_a)
        push(step, side_a, 3, False, to_b)
        across(step, side_a)

    def event_b(step, which):
        zz = column(step)
        arrived(zz, which)
        across(step, which)

    def ready(step):
        for t in partners:
            zz = column_of(step, t)
            for ss in (side, side_a, side_b, side_ab):
                remote(slot(zz, ss, t), slot(zz, ss, t), send_t.at[t, zz, ss], recv_t.at[t, zz, ss], (me, t)).wait_recv()

    event_z(0)
    hbuf[mine] = h_ref[...]
    buf[mine, z, pl.ds(pl.multiple_of(side * period, period), period), :] = packed_ref[...]
    acc[...] = jnp.zeros_like(acc)
    top[...] = jnp.full(top.shape, -1e38, F32)
    total[...] = jnp.zeros_like(total)
    for t in partners:
        remote(h_ref, hbuf.at[t], send_h.at[t], recv_h.at[t], (me, t)).wait_recv()

    tokens = n_tp * rows
    piece = hbuf[...].reshape(tokens, hbuf.shape[2])
    loads[0].wait()
    turned = jnp.dot(piece, qr_ref[...], preferred_element_type=F32)
    copies = turned.shape[1] // LANES
    turned = rotate(
        turned, jnp.concatenate([cos_ref[...]] * copies, axis=1), jnp.concatenate([sin_ref[...]] * copies, axis=1)
    ).astype(BF16)
    loads[1].wait()
    for head in range(heads):
        q[head, :, :nope] = jnp.dot(
            piece, qn_ref[:, head * nope : (head + 1) * nope], preferred_element_type=F32
        ).astype(BF16)
        q[head, :, nope : nope + rope] = turned[:, head * rope : (head + 1) * rope]
        q[head, :, nope + rope :] = jnp.broadcast_to(
            bias_ref[head : head + 1, :], (tokens, LANES - rope)
        )

    def attend(step, beside):
        places = [(t, column_of(step, t)) for t in range(n_tp)]

        def one(head, _):
            at = pl.ds(pl.multiple_of(head * nope, nope), nope)
            weight = jnp.concatenate([ku_ref[:, at], vu_ref[:, at]], axis=1)
            latents = jnp.concatenate([buf[t, zz, :, :rank] for t, zz in places], axis=0)
            extra = jnp.concatenate([buf[t, zz, :, rank:] for t, zz in places], axis=0)
            both = jnp.dot(latents, weight, preferred_element_type=F32).astype(BF16)
            keys = jnp.concatenate([both[:, :nope], extra], axis=1)
            scores = lax.dot_general(q[head], keys, (((1,), (1,)), ((), ())), preferred_element_type=F32)
            old = top[head][:, :1]
            new = jnp.maximum(old, jnp.max(scores, axis=-1, keepdims=True))
            weights = jnp.exp2((scores - new) * (factor * LOG2E))
            fade = jnp.exp2((old - new) * (factor * LOG2E))
            top[head] = jnp.broadcast_to(new, top.shape[1:])
            total[head] = total[head] * fade + jnp.sum(weights, axis=-1, keepdims=True)
            acc[head] = acc[head] * fade + jnp.dot(
                weights.astype(BF16), both[:, nope:], preferred_element_type=F32
            )
            return 0

        together = next(n for n in (4, 2, 1) if heads % n == 0)
        turns = heads // together

        def some(i, _):
            for k, event in enumerate(beside):
                pl.when(i == k * turns // len(beside))(event)
            for j in range(together):
                one(i * together + j, 0)
            return 0

        lax.fori_loop(0, turns, some, 0)

    event_a(0)
    event_z(order[1])
    event_b(0, side_b)
    event_b(0, side_ab)
    ready(0)
    loads[2].wait()
    loads[3].wait()
    for i, step in enumerate(order):
        if i + 1 < len(order):
            later = order[i + 1]
            attend(
                step,
                [
                    functools.partial(event_a, later),
                    functools.partial(event_b, later, side_b),
                    functools.partial(event_b, later, side_ab),
                ]
                + [functools.partial(event_z, step) for step in order[i + 2 : i + 3]],
            )
            ready(later)
        else:
            attend(step, [])
    loads[4].wait()

    for head in range(heads):
        att[:, head * nope : (head + 1) * nope] = (acc[head] / total[head]).astype(BF16)

    for t in partners:
        lines = pl.ds(pl.multiple_of(t * rows, rows), rows)
        outbox[t] = jnp.dot(att[lines, :], wo_ref[...], preferred_element_type=F32).astype(BF16)
        copy = remote(outbox.at[t], inbox.at[mine], send_o.at[t], recv_o.at[mine], (me, t))
        copy.start()
        started.append(lambda copy=copy: copy)
    lines = pl.ds(pl.multiple_of(mine * rows, rows), rows)
    branch = jnp.dot(att[lines, :], wo_ref[...], preferred_element_type=F32).astype(BF16).astype(F32)
    for t in partners:
        remote(outbox.at[t], inbox.at[t], send_o.at[t], recv_o.at[t], (me, t)).wait_recv()
        branch = branch + inbox[t].astype(F32)
    out_ref[...] = (latent_ref[...].astype(F32) + gate_ref[...] * branch).astype(BF16)
    for make in started:
        make().wait_send()


def tables(positions, rope, real):
    quarter = rope // 4
    lane = jnp.arange(LANES, dtype=jnp.int32)
    pair = (lane % rope) // 2
    inverse = ROPE_BASE ** (-(pair % quarter).astype(F32) / quarter)
    place = jnp.where(pair[None, :] < quarter, (positions // GRID_W)[:, None], (positions % GRID_W)[:, None])
    angle = jnp.where(real[:, None], place.astype(F32) * inverse[None, :], 0.0)
    sine = jnp.sin(angle)
    return jnp.cos(angle), jnp.where(lane[None, :] % 2 == 0, -sine, sine)


def body(
    latent, cond, ctx_mod, context, shift_w, scale_w, gate_w, norm_gain, w_qn, w_qr, w_kv_down, w_rope_key,
    kv_gain, w_key_up, w_value_up, ctx_bias, w_out,
):
    n_sp, n_tp = lax.axis_size("sp"), lax.axis_size("tp")
    sp_index, tp_index = lax.axis_index("sp"), lax.axis_index("tp")
    rows, width = latent.shape
    ctx_rows = context.shape[0]
    tokens = rows * n_tp
    heads = ctx_bias.shape[0]
    nope = w_key_up.shape[1] // heads
    rope = w_rope_key.shape[1]
    rank = w_kv_down.shape[1]
    period = -(-(rows + ctx_rows) // 16) * 16
    factor = (nope + rope) ** (-0.5)
    feat = shift_w.shape[0]
    pair = jnp.stack([jax.nn.silu(cond), jax.nn.silu(ctx_mod)])
    pair = lax.dynamic_slice_in_dim(pair, sp_index * feat, feat, 1)
    pair = jnp.concatenate([pair, jnp.zeros((6, feat), F32)], axis=0)
    pad = jnp.zeros((period - rows - ctx_rows, width), BF16)
    x = jnp.concatenate([latent, context, pad], axis=0)
    line = jnp.arange(period, dtype=jnp.int32)
    own_cos, own_sin = tables(sp_index * tokens + tp_index * rows + line, rope, line < rows)
    place = jnp.arange(tokens, dtype=jnp.int32)
    cosine, sine = tables(sp_index * tokens + place, rope, place >= 0)

    vmem = pl.BlockSpec(memory_space=pltpu.VMEM)
    dma = pltpu.SemaphoreType.DMA
    h, packed, gate = pl.pallas_call(
        functools.partial(modulation_kernel, n_sp, n_tp, rows, ctx_rows),
        out_shape=(
            jax.ShapeDtypeStruct((rows, width), BF16),
            jax.ShapeDtypeStruct((period, rank + LANES), BF16),
            jax.ShapeDtypeStruct((1, width), F32),
        ),
        in_specs=[vmem] * 11,
        out_specs=(vmem,) * 3,
        scratch_shapes=[
            pltpu.VMEM((n_sp, 8, LANES), F32),
            pltpu.VMEM((n_sp, 8, LANES), F32),
            pltpu.VMEM((8, LANES), F32),
            pltpu.VMEM((n_sp * n_tp, 8, LANES), F32),
            pltpu.VMEM((8, width), F32),
            dma((n_sp,)),
            dma((n_sp,)),
            dma((n_sp * n_tp,)),
            dma((n_sp * n_tp,)),
        ],
        compiler_params=pltpu.CompilerParams(
            collective_id=0, has_side_effects=True, vmem_limit_bytes=40 * 1024 * 1024
        ),
        name="modulation",
    )(
        pair, shift_w, scale_w, gate_w, x, norm_gain[None, :], w_kv_down, w_rope_key, kv_gain[None, :],
        own_cos, own_sin,
    )

    scaled = ctx_bias / factor
    high = lax.reduce_precision(scaled, 8, 7)
    middle = lax.reduce_precision(scaled - high, 8, 7)
    low = scaled - high - middle
    bias = jnp.stack([high, middle, low, jnp.full_like(scaled, -1e30)], axis=1)
    bias = jnp.concatenate([bias, jnp.zeros((heads, LANES - rope - FLAGS), F32)], axis=1).astype(BF16)
    short = -(heads * rope) % LANES
    if short:
        w_qr = jnp.concatenate([w_qr, jnp.zeros((width, short), BF16)], axis=1)

    nz = n_sp // 4
    return pl.pallas_call(
        functools.partial(attention_kernel, n_sp, n_tp, heads, nope, rope, factor),
        out_shape=jax.ShapeDtypeStruct((rows, width), BF16),
        in_specs=[vmem] * 5 + [pl.BlockSpec(memory_space=pl.ANY)] * 5 + [vmem] * 2,
        out_specs=vmem,
        scratch_shapes=[
            pltpu.VMEM(w_qr.shape, BF16),
            pltpu.VMEM(w_qn.shape, BF16),
            pltpu.VMEM(w_key_up.shape, BF16),
            pltpu.VMEM(w_value_up.shape, BF16),
            pltpu.VMEM(w_out.shape, BF16),
            dma((5,)),
            pltpu.VMEM((n_tp, nz, 4 * period, rank + LANES), BF16),
            pltpu.VMEM((n_tp, rows, width), BF16),
            pltpu.VMEM((heads, tokens, nope + LANES), BF16),
            pltpu.VMEM((heads, tokens, nope), F32),
            pltpu.VMEM((heads, tokens, LANES), F32),
            pltpu.VMEM((heads, tokens, LANES), F32),
            pltpu.VMEM((tokens, heads * nope), BF16),
            pltpu.VMEM((n_tp, rows, width), BF16),
            pltpu.VMEM((n_tp, rows, width), BF16),
            dma((4, nz, 4)),
            dma((nz, 4)),
            dma((n_tp, nz, 4)),
            dma((n_tp, nz, 4)),
            dma((n_tp,)),
            dma((n_tp,)),
            dma((n_tp,)),
            dma((n_tp,)),
        ],
        compiler_params=pltpu.CompilerParams(
            collective_id=1, has_side_effects=True, vmem_limit_bytes=60 * 1024 * 1024
        ),
        name="attention",
    )(h, packed, bias, cosine, sine, w_qn, w_qr, w_key_up, w_value_up, w_out, latent, gate)


def solution(mesh):
    placed = (
        P(("sp", "tp"), None),
        P(),
        P(),
        P(("sp", "tp"), None),
        P("sp", "tp"),
        P("sp", "tp"),
        P("sp", "tp"),
        P(),
        P(None, "tp"),
        P(None, "tp"),
        P(),
        P(),
        P(),
        P(None, "tp"),
        P(None, "tp"),
        P("tp"),
        P("tp", None),
    )
    return jax.shard_map(
        body, mesh=mesh, in_specs=placed, out_specs=P(("sp", "tp"), None), check_vma=False
    )
```

profile of v0, /device:TPU:1, one launch (start us, length us, event | category | flops | bytes accessed | tf_op | source)
XLA Modules:
  0.0 97.8 jit_solution(1619178674030687626)
XLA Ops:
  0.0 0.0 copy-start.6
  0.0 0.0 copy-start.8
  0.0 0.0 copy-start
  0.1 0.4 negate_select_fusion.1
  0.5 0.9 divide_multiply_fusion.1
  1.4 0.7 divide_multiply_fusion
  2.1 0.1 fusion.2
  2.2 1.1 %pad_maximum_fusion.x_ref = bf16[144,2048]{1,0:T(8,128)(2,1)S(1)} fusion(bf16[16,2048]{1,0:T(8,128)(2,1)} %param.20, bf16[128,2048]{1,0:T(8,128)(2,1)} %latent_ref.1), kind=kLoop, calls=%fused_computation | loop fusion | flops 1179648 | bytes 1179648 | tf_op jit(solution)/shard_map/concatenate | solution.py:386
  3.3 1.3 %copy.18.rope_ref = bf16[2048,64]{1,0:T(8,128)(2,1)S(1)} copy(bf16[2048,64]{0,1:T(8,128)(2,1)} %param.28) | data formatting | bytes 524288 | tf_op args[11]
  4.6 0.0 copy-done.6
  4.6 0.0 copy-done.8
  4.6 0.0 copy-done
  4.6 0.0 copy-start.2
  4.6 1.0 %copy-done.2 = f32[128,1024]{1,0:T(8,128)S(1)} copy-done((f32[128,1024]{1,0:T(8,128)S(1)}, f32[128,1024]{1,0:T(8,128)}, u32[]{:S(2)}) %copy-start.2) | copy-done | bytes 524312
  5.7 0.0 copy-start.3
  5.7 1.0 %copy-done.3 = f32[128,1024]{1,0:T(8,128)S(1)} copy-done((f32[128,1024]{1,0:T(8,128)S(1)}, f32[128,1024]{1,0:T(8,128)}, u32[]{:S(2)}) %copy-start.3) | copy-done | bytes 524312
  6.7 0.0 copy-start.4
  6.7 1.0 %copy-done.4 = f32[128,1024]{1,0:T(8,128)S(1)} copy-done((f32[128,1024]{1,0:T(8,128)S(1)}, f32[128,1024]{1,0:T(8,128)}, u32[]{:S(2)}) %copy-start.4) | copy-done | bytes 524312
  7.7 0.0 copy-start.9
  7.7 17.6 %modulation.1 = (bf16[128,2048]{1,0:T(8,128)(2,1)S(1)}, bf16[144,640]{1,0:T(8,128)(2,1)S(1)}, f32[1,2048]{1,0:T(1,128)S(1)}) custom-call(f32[8,128]{1,0:T(8,128)S(1)} %concatenate.10.pair_ref, f32[128,1024]{1,0:T(8,128)S(1)} %copy-done.2, f32[128,1024]{1,0:T(8,128)S(1)} %copy-done.3, f32[128,1024]{1,0:T(8,128)S(1)} %copy-done.4, ...), custom_call_target="tpu_custom_call" | custom-call | tf_op jit(solution)/shard_map/modulation/pallas_call | solution.py:394
  25.4 0.0 copy-start.1
  25.4 0.8 copy-done.1
  26.2 0.7 copy-done.5
  26.8 0.6 copy-done.7
  27.4 1.3 %negate_select_fusion = (f32[256,128]{1,0:T(8,128)}, f32[256,128]{1,0:T(8,128)}) fusion(f32[128]{0:T(128)S(1)} %fusion.12, s32[256]{0:T(256)S(1)} %get-tuple-element.20, s32[256]{0:T(256)S(1)} %get-tuple-element.21, pred[128]{0:T(512)(128)(4,1)S(1)} %get-tuple-element.18, pred[128]{0:T(512)(128)(4,1)S(1)} %get-tuple-element.19), kind=kLoop, calls=%fused_computation.1 | loop fusion | flops 163840 | bytes 264960 | tf_op jit(solution)/shard_map/jit(_where)/select_n | solution.py:363
  28.7 0.0 copy-done.9
  28.7 0.1 copy.19
  28.8 0.1 copy.20
  28.9 0.1 copy.21
  29.0 0.7 concatenate.12.bias_ref
  29.7 66.2 %attention.1 = bf16[128,2048]{1,0:T(8,128)(2,1)} custom-call(bf16[128,2048]{1,0:T(8,128)(2,1)} %copy-done.1, bf16[144,640]{1,0:T(8,128)(2,1)} %copy-done.5, bf16[8,64]{1,0:T(8,128)(2,1)} %concatenate.12.bias_ref, f32[256,128]{1,0:T(8,128)} %get-tuple-element.14.cos_ref, f32[256,128]{1,0:T(8,128)} %get-tuple-element.13.sin_ref, bf16[2048,1024]{1,0:T(8,128)(2,1)} %qn_hbm.1, ...), custom_call_target="tpu_custom_call" | custom-call | tf_op jit(solution)/shard_map/attention/pallas_call | solution.py:434
  95.9 1.9 %copy.23 = bf16[128,2048]{1,0:T(8,128)(2,1)} copy(bf16[128,2048]{1,0:T(8,128)(2,1)} %attention.1) | data formatting | bytes 1048576
  (11 shorter events, 0.1 us)
Async XLA Ops:
  0.0 4.6 %copy-start.6 = (f32[2048]{0:T(1024)S(1)}, f32[2048]{0:T(1024)}, u32[]{:S(2)}) copy-start(f32[2048]{0:T(1024)} %param.24) | copy-start | bytes 24580
  0.0 4.6 %copy-start.8 = (f32[512]{0:T(512)S(1)}, f32[512]{0:T(512)}, u32[]{:S(2)}) copy-start(f32[512]{0:T(512)} %param.29) | copy-start | bytes 6148
  0.0 4.6 %copy-start = (bf16[2048,512]{1,0:T(8,128)(2,1)S(1)}, bf16[2048,512]{1,0:T(8,128)(2,1)}, u32[]{:S(2)}) copy-start(bf16[2048,512]{1,0:T(8,128)(2,1)} %down_ref.1) | copy-start | bytes 6291460
  4.6 1.0 %copy-start.2 = (f32[128,1024]{1,0:T(8,128)S(1)}, f32[128,1024]{1,0:T(8,128)}, u32[]{:S(2)}) copy-start(f32[128,1024]{1,0:T(8,128)} %shift_w.1) | copy-start | bytes 1572868
  5.7 1.0 %copy-start.3 = (f32[128,1024]{1,0:T(8,128)S(1)}, f32[128,1024]{1,0:T(8,128)}, u32[]{:S(2)}) copy-start(f32[128,1024]{1,0:T(8,128)} %scale_w.1) | copy-start | bytes 1572868
  6.7 1.0 %copy-start.4 = (f32[128,1024]{1,0:T(8,128)S(1)}, f32[128,1024]{1,0:T(8,128)}, u32[]{:S(2)}) copy-start(f32[128,1024]{1,0:T(8,128)} %gate_w.1) | copy-start | bytes 1572868
  7.7 21.0 %copy-start.9 = (f32[8]{0:T(128)S(1)}, f32[8]{0:T(128)}, u32[]{:S(2)}) copy-start(f32[8]{0:T(128)} %param.32) | copy-start | bytes 100
  25.4 0.8 copy-start.1
  26.2 0.7 copy-start.5
  26.8 0.6 copy-start.7
where the time goes:
time: 98.2 us; the launch traced here: 97.8 us
  Pallas kernels  83.8 us (85%)
  local copies, waits for them, and re-layouts  9.3 us (9%)
  other arithmetic  4.54 us (5%)
    pallas_call x1, Pallas kernels, body(): pl.pallas_call(functools.partial(attention_kernel, n_sp, n_tp, heads, nop...  66.2 us
    pallas_call x1, Pallas kernels, body(): pl.pallas_call(functools.partial(modulation_kernel, n_sp, n_tp, rows, ctx...  17.6 us
    unnamed x22, local copies, waits for them, and re-layouts  8.33 us

commit v1 on v0

v1 whole, which is shorter than its diff:
```python
import functools

import jax
import jax.numpy as jnp
import numpy as np
from jax import lax
from jax.experimental import pallas as pl
from jax.experimental.pallas import tpu as pltpu
from jax.sharding import PartitionSpec as P

GRID_W = 128
EPS = 1e-06
ROPE_BASE = 10000.0
LANES = 128
LOG2E = 1.4426950408889634
MODS = 5
MESH = pl.DeviceIdType.MESH
F32 = jnp.float32
BF16 = jnp.bfloat16


def remote(src, dst, send, recv, device):
    return pltpu.make_async_remote_copy(
        src_ref=src, dst_ref=dst, send_sem=send, recv_sem=recv, device_id=device, device_id_type=MESH
    )


def rotate(values, cosine, sine):
    width = values.shape[-1]
    ahead = pltpu.roll(values, width - 1, 1)
    behind = pltpu.roll(values, 1, 1)
    even = lax.broadcasted_iota(jnp.int32, values.shape, 1) % 2 == 0
    return values * cosine + jnp.where(even, ahead, behind) * sine


def dot(a, b):
    return jnp.dot(a, b, preferred_element_type=F32)


def dot_nt(a, b):
    return lax.dot_general(a, b, (((1,), (1,)), ((), ())), preferred_element_type=F32)


class Slot:
    def __init__(self, rows, ctx_rows, rank):
        self.split = 2 if rows % 32 == 0 else 1
        self.rows = rows
        self.ctx = -(-ctx_rows // 16) * 16
        self.columns = rank // LANES
        self.rope_at = self.columns * rows
        self.rope_rows = rows // self.split
        self.ctx_at = self.rope_at + self.rope_rows
        self.ctx_rope_at = self.ctx_at + self.columns * self.ctx
        self.height = self.ctx_rope_at + self.ctx

    def planes(self, n_tp, nz):
        return max(1, min(nz, 512 // (self.ctx * 4 * n_tp)))


def kernel(
    n_sp, n_tp, heads, nope, rope, ctx_rows, factor, slot_of,
    cond_hbm, ctxm_hbm, shift_hbm, scale_hbm, gate_hbm, latent_hbm, context_hbm, gain_hbm, down_hbm, rope_hbm,
    kvg_hbm, rowtab_hbm, coltab_hbm, bias_hbm, qr_hbm, qn_hbm, ku_hbm, vu_hbm, wo_hbm,
    out_ref,
    cond_v, ctxm_v, shift_v, scale_v, gate_v, x_v, ctx_v, gain_v, down_v, rope_v, kvg_v, rowtab_v, coltab_v, bias_v,
    qr_v, qn_v, ku_v, vu_v, wo_v, load_sem,
    part, landed, reduced, full, mods, normed, hown, hfull, cos_v, sin_v, vut, bias_b,
    buf, qt, kbuf, vt, acc, top, total_v, att, outbox, inbox,
    send1, recv1, send2, recv2, send_x, recv_x, send, recv, send_t, recv_t, send_o, recv_o,
):
    me = lax.axis_index("sp")
    mine = lax.axis_index("tp")
    total = n_sp * n_tp
    flat = me * n_tp + mine
    barrier = pltpu.get_barrier_semaphore()
    rows, rank = slot_of.rows, ku_v.shape[0]
    depth = x_v.shape[2]
    tokens = n_tp * rows
    partners = [lax.rem(mine + i, n_tp) for i in range(1, n_tp)]

    pairs = dict(
        cond=(cond_hbm, cond_v), ctxm=(ctxm_hbm, ctxm_v), shift=(shift_hbm, shift_v), scale=(scale_hbm, scale_v),
        gate=(gate_hbm, gate_v), x=(latent_hbm, x_v.at[mine]), ctx=(context_hbm, ctx_v), gain=(gain_hbm, gain_v),
        down=(down_hbm, down_v), rope=(rope_hbm, rope_v), kvg=(kvg_hbm, kvg_v), rowtab=(rowtab_hbm, rowtab_v),
        coltab=(coltab_hbm, coltab_v), bias=(bias_hbm, bias_v), qr=(qr_hbm, qr_v), qn=(qn_hbm, qn_v),
        ku=(ku_hbm, ku_v), vu=(vu_hbm, vu_v), wo=(wo_hbm, wo_v),
    )
    loads = {
        name: pltpu.make_async_copy(src, dst, load_sem.at[i]) for i, (name, (src, dst)) in enumerate(pairs.items())
    }
    late = ("qr", "qn", "ku", "vu", "wo")
    for name in loads:
        if name not in late:
            loads[name].start()

    part[...] = jnp.zeros_like(part)
    landed[...] = jnp.zeros_like(landed)

    def greet(i, _):
        other = lax.rem(flat + i, total)
        pl.semaphore_signal(barrier, inc=1, device_id=(other // n_tp, other % n_tp), device_id_type=MESH)
        return 0

    lax.fori_loop(1, total, greet, 0)

    feat, columns = shift_v.shape
    blocks = columns // LANES
    per = -(-MODS * blocks // n_sp)
    sides = []
    for name, ref in (("cond", cond_v), ("ctxm", ctxm_v)):
        loads[name].wait()
        value = ref[pl.ds(me, 1), :]
        value = value / (1.0 + jnp.exp(-value))
        sides.append(jnp.broadcast_to(value, (LANES, feat)).T)
    plan = ((shift_v, 0, "shift"), (shift_v, 1, None), (scale_v, 0, "scale"), (scale_v, 1, None), (gate_v, 0, "gate"))
    for row, (weight, which, name) in enumerate(plan):
        if name:
            loads[name].wait()
        for block in range(blocks):
            unit = row * blocks + block
            part[unit // per, unit % per : unit % per + 1, :] = jnp.sum(
                weight[:, block * LANES : (block + 1) * LANES] * sides[which], axis=0, keepdims=True
            )
    for name in late:
        loads[name].start()
    pl.semaphore_wait(barrier, total - 1)

    some = pl.ds(0, per)

    def scattering(other):
        return remote(part.at[other, some], landed.at[me, some], send1.at[other], recv1.at[me], (other, mine))

    def scatter(i, _):
        scattering(lax.rem(me + i, n_sp)).start()
        return 0

    lax.fori_loop(1, n_sp, scatter, 0)
    loads["x"].wait()
    swaps = [remote(x_v.at[mine], x_v.at[mine], send_x.at[t], recv_x.at[mine], (me, t)) for t in partners]
    for swap in swaps:
        swap.start()
    landed[me] = part[me]

    loads["gain"].wait()
    loads["ctx"].wait()
    gain = gain_v[...]

    def norm(values):
        values = values.astype(F32)
        return values * lax.rsqrt(jnp.mean(values * values, axis=-1, keepdims=True) + EPS) * gain

    ctx = slot_of.ctx
    normed[:rows] = norm(x_v[mine])
    padded = ctx_v[...]
    if ctx != ctx_rows:
        padded = jnp.concatenate([padded.astype(F32), jnp.zeros((ctx - ctx_rows, depth), F32)], axis=0)
    normed[rows:] = norm(padded)

    loads["rowtab"].wait()
    loads["coltab"].wait()
    for k in range(tokens // GRID_W):
        line = pl.ds(me * (tokens // GRID_W) + k, 1)
        at = slice(k * GRID_W, (k + 1) * GRID_W)
        cos_v[at] = coltab_v[0] + rowtab_v[0, line]
        sin_v[at] = coltab_v[1] + rowtab_v[1, line]

    def scattered(i, _):
        other = lax.rem(me + i, n_sp)
        remote(part.at[other, some], landed.at[other, some], send1.at[other], recv1.at[other], (other, mine)).wait()
        return 0

    lax.fori_loop(1, n_sp, scattered, 0)
    reduced[...] = jnp.sum(landed[...], axis=0)

    def gather(i, _):
        other = lax.rem(flat + i, total)
        remote(
            reduced.at[some], full.at[flat, some], send2.at[other], recv2.at[flat], (other // n_tp, other % n_tp)
        ).start()
        return 0

    lax.fori_loop(1, total, gather, 0)
    full[flat] = reduced[...]

    loads["vu"].wait()
    for at in range(0, vu_v.shape[1], LANES):
        vut[at : at + LANES, :] = vu_v[:, at : at + LANES].T
    loads["bias"].wait()
    for head in range(heads):
        bias_b[head] = jnp.broadcast_to(bias_v[:, head : head + 1] * LOG2E, bias_b.shape[1:])
    acc[...] = jnp.zeros_like(acc)
    top[...] = jnp.full(top.shape, -1e30, F32)
    total_v[...] = jnp.zeros_like(total_v)
    loads["down"].wait()
    loads["rope"].wait()
    loads["kvg"].wait()

    def gathered(i, _):
        other = lax.rem(flat + i, total)
        remote(
            reduced.at[some], full.at[other, some], send2.at[other], recv2.at[other], (other // n_tp, other % n_tp)
        ).wait()
        return 0

    lax.fori_loop(1, total, gathered, 0)
    for unit in range(MODS * blocks):
        row, block = unit // blocks, unit % blocks
        for t in range(n_tp):
            at = t * columns + block * LANES
            mods[row : row + 1, at : at + LANES] = full[(unit // per) * n_tp + t, unit % per : unit % per + 1, :]

    def modulate(values, which):
        return (values * (1.0 + mods[2 + which : 3 + which, :]) + mods[which : which + 1, :]).astype(BF16)

    hown[:rows] = modulate(normed[:rows], 0)
    hown[rows:] = modulate(normed[rows:], 1)
    h = hown[...]
    inner = dot(h, down_v[...])
    inner = inner * lax.rsqrt(jnp.mean(inner * inner, axis=-1, keepdims=True) + EPS)
    inner = (inner * kvg_v[...]).astype(BF16)
    key = dot_nt(h, rope_v[...])
    key = jnp.concatenate([key, jnp.zeros((key.shape[0], LANES - rope), F32)], axis=1)
    own_rows = pl.ds(pl.multiple_of(mine * rows, rows), rows)
    turned = rotate(key[:rows], cos_v[own_rows], sin_v[own_rows])

    nz = n_sp // 4
    z, side = me // 4, me % 4
    y, x = side // 2, side % 2
    odd = mine % 2
    flip_x = y * 2 + (1 - x)
    flip_y = (1 - y) * 2 + x
    side_a = flip_x * (1 - odd) + flip_y * odd
    side_b = flip_y * (1 - odd) + flip_x * odd
    side_ab = 3 - side

    own = (mine, z, side)
    for c in range(slot_of.columns):
        lanes = slice(c * LANES, (c + 1) * LANES)
        buf[mine, z, side, c * rows : (c + 1) * rows] = inner[:rows, lanes]
        at = slot_of.ctx_at + c * ctx
        buf[mine, z, side, at : at + ctx] = inner[rows:, lanes]
    shared = turned[: slot_of.rope_rows]
    if slot_of.split == 2:
        shared = shared + pltpu.roll(turned[slot_of.rope_rows :], rope, 1)
    buf[mine, z, side, slot_of.rope_at : slot_of.ctx_at] = shared.astype(BF16)
    buf[mine, z, side, slot_of.ctx_rope_at :] = key[rows:].astype(BF16)

    def plane(step, t):
        sign = 1 - 2 * (1 - t % 2)
        reach = jnp.minimum(z, nz - 1 - z)
        away = (step + 1) // 2
        near = z + (2 * (step % 2) - 1) * sign * away
        low = z <= nz - 1 - z
        far = lax.select(low, z * 0 + step, z * 0 + (nz - 1) - step)
        return lax.select(reach * 2 >= step, near, far)

    def slot(t, zz, ss):
        return buf.at[t, zz, ss]

    def peer(zz, ss):
        return (zz * 4 + ss, mine)

    def link(zz, ss, way, device):
        return remote(slot(mine, zz, ss), slot(mine, zz, ss), send.at[way, zz, ss], recv.at[zz, ss], device)

    def push(zz, ss, way, device, when=None):
        if when is None:
            link(zz, ss, way, device).start()
        else:
            pl.when(when)(lambda: link(zz, ss, way, device).start())

    def pushed(zz, ss, way, when=None):
        wait = lambda: link(zz, ss, way, peer(z, side_a)).wait_send()
        if when is None:
            wait()
        else:
            pl.when(when)(wait)

    def over(zz, ss, t):
        return remote(slot(mine, zz, ss), slot(mine, zz, ss), send_t.at[t, zz, ss], recv_t.at[mine, zz, ss], (me, t))

    def across(zz, ss):
        for t in partners:
            over(zz, ss, t).start()

    def arrived(zz, ss):
        link(zz, ss, 0, peer(z, side_a)).wait_recv()

    up, down = peer(lax.rem(z + 1, nz), side), peer(lax.rem(z + nz - 1, nz), side)
    to_a, to_b = peer(z, side_a), peer(z, side_b)

    def event_z(step):
        zz = plane(step, mine)
        if step == 0:
            push(zz, side, 3, to_b)
            push(zz, side, 2, to_a)
            push(zz, side, 0, up, z < nz - 1)
            push(zz, side, 1, down, z > 0)
        else:
            arrived(zz, side)
            push(zz, side, 0, up, (zz < z) & (z < nz - 1))
            push(zz, side, 1, down, (zz > z) & (z > 0))
            push(zz, side, 2, to_a)
            push(zz, side, 3, to_b)
        across(zz, side)

    def event_a(step):
        zz = plane(step, mine)
        arrived(zz, side_a)
        push(zz, side_a, 3, to_b)
        across(zz, side_a)

    def event_b(step, which):
        zz = plane(step, mine)
        arrived(zz, which)
        across(zz, which)

    def sent():
        for step in range(nz):
            zz = plane(step, mine)
            pushed(zz, side, 2)
            pushed(zz, side, 3)
            pushed(zz, side_a, 3)
            pushed(zz, side, 0, (zz <= z) & (z < nz - 1))
            pushed(zz, side, 1, (zz >= z) & (z > 0))
            for ss in (side, side_a, side_b, side_ab):
                for t in partners:
                    over(zz, ss, t).wait_send()

    event_z(0)

    hfull[mine] = hown[:rows]
    for t in partners:
        remote(x_v.at[t], x_v.at[t], send_x.at[t], recv_x.at[t], (me, t)).wait_recv()
        hfull[t] = modulate(norm(x_v[t]), 0)
    piece = hfull[...].reshape(tokens, depth)
    loads["qr"].wait()
    turned = dot(piece, qr_v[...])
    copies = turned.shape[1] // LANES
    turned = rotate(turned, jnp.concatenate([cos_v[...]] * copies, axis=1), jnp.concatenate([sin_v[...]] * copies, axis=1))
    turned = (turned * (factor * LOG2E)).T.astype(BF16)
    blank = jnp.zeros((LANES - rope, tokens), BF16)
    for head in range(heads):
        mine_rope = turned[head * rope : (head + 1) * rope]
        for g in range(slot_of.split):
            both = [mine_rope, blank] if g == 0 else [blank, mine_rope]
            qt[head, g, nope:, :] = jnp.concatenate(both, axis=0)
    loads["qn"].wait()
    wide = min(2 * nope, heads * nope)
    for at in range(0, heads * nope, wide):
        flatq = dot(piece, qn_v[:, at : at + wide]) * (factor * LOG2E)
        for k in range(wide // nope):
            value = flatq[:, k * nope : (k + 1) * nope].T.astype(BF16)
            for g in range(slot_of.split):
                qt[at // nope + k, g, :nope, :] = value
    loads["ku"].wait()

    def process(lat, ropes, biased=False, valid=None):
        count = lat.shape[0]
        piece_rows = count // len(ropes)
        for at in range(0, heads * nope, wide):
            kbuf[:count, at : at + wide] = dot(lat, ku_v[:, at : at + wide]).astype(BF16)
            vt[at : at + wide, :count] = dot_nt(vut[at : at + wide, :], lat).astype(BF16)
        for head in range(heads):
            pieces = []
            for g, rope_rows in enumerate(ropes):
                keys = jnp.concatenate(
                    [kbuf[g * piece_rows : (g + 1) * piece_rows, head * nope : (head + 1) * nope], rope_rows], axis=1
                )
                pieces.append(dot(keys, qt[head, g]))
            scores = jnp.concatenate(pieces, axis=0)
            if valid is not None:
                scores = jnp.where(valid, scores, -1e30)
            old = top[head][:1]
            high = jnp.max(scores, axis=0, keepdims=True)
            if biased:
                high = high + bias_b[head][:1]
            new = jnp.maximum(old, high)
            less = new - bias_b[head][:1] if biased else new
            weights = jnp.exp2(scores - less)
            fade = jnp.exp2(old - new)
            top[head] = jnp.broadcast_to(new, top.shape[1:])
            total_v[head] = total_v[head] * fade + jnp.sum(weights, axis=0, keepdims=True)
            acc[head] = acc[head] * fade + dot(vt[head * nope : (head + 1) * nope, :count], weights.astype(BF16))

    def chunk(k):
        step, half = k // 2, k % 2
        pair = (
            jnp.where(half == 0, side, flip_y),
            jnp.where(half == 0, flip_x, side_ab),
        )
        places = [(t, plane(step, t), ss) for t in range(n_tp) for ss in pair]
        for t in partners:
            zz = plane(step, t)
            for ss in pair:
                remote(slot(t, zz, ss), slot(t, zz, ss), send_t.at[t, zz, ss], recv_t.at[t, zz, ss], (me, t)).wait_recv()
        tall = slot_of.rope_rows

        def block(place, c, g):
            t, zz, ss = place
            return buf[t, zz, ss, c * rows + g * tall : c * rows + (g + 1) * tall]

        lat = jnp.concatenate(
            [
                jnp.concatenate([block(place, c, g) for g in range(slot_of.split) for place in places], axis=0)
                for c in range(slot_of.columns)
            ],
            axis=1,
        )
        ropes = jnp.concatenate(
            [buf[t, zz, ss, slot_of.rope_at : slot_of.ctx_at] for t, zz, ss in places], axis=0
        )
        process(lat, [ropes] * slot_of.split)

    def before(k):
        if k < nz:
            event_a(k)
        if k + 1 < nz:
            event_z(k + 1)
        event_b(k // 2, side_b if k % 2 == 0 else side_ab)

    def turn(k, _):
        for i in range(2 * nz):
            pl.when(k == i)(functools.partial(before, i))
        chunk(k)
        return 0

    lax.fori_loop(0, 2 * nz, turn, 0)

    per_plane = slot_of.planes(n_tp, nz)

    def context_chunk(i, _):
        places = [
            (t, i * per_plane + dz, ss) for t in range(n_tp) for dz in range(per_plane) for ss in range(4)
        ]
        lat = jnp.concatenate(
            [
                jnp.concatenate(
                    [
                        buf[t, zz, ss, slot_of.ctx_at + c * ctx : slot_of.ctx_at + (c + 1) * ctx]
                        for t, zz, ss in places
                    ],
                    axis=0,
                )
                for c in range(slot_of.columns)
            ],
            axis=1,
        )
        ropes = jnp.concatenate([buf[t, zz, ss, slot_of.ctx_rope_at :] for t, zz, ss in places], axis=0)
        valid = None
        if ctx != ctx_rows:
            valid = lax.broadcasted_iota(jnp.int32, (lat.shape[0], tokens), 0) % ctx < ctx_rows
        process(lat, [ropes], True, valid)
        return 0

    if nz // per_plane == 1:
        context_chunk(0, 0)
    else:
        lax.fori_loop(0, nz // per_plane, context_chunk, 0)

    for head in range(heads):
        att[:, head * nope : (head + 1) * nope] = (acc[head] / total_v[head][:1]).T.astype(BF16)
    loads["wo"].wait()
    shipped = []
    for t in partners:
        lines = pl.ds(pl.multiple_of(t * rows, rows), rows)
        outbox[t] = dot(att[lines, :], wo_v[...]).astype(BF16)
        copy = remote(outbox.at[t], inbox.at[mine], send_o.at[t], recv_o.at[mine], (me, t))
        copy.start()
        shipped.append(copy)
    branch = dot(att[own_rows, :], wo_v[...]).astype(BF16).astype(F32)
    for t in partners:
        remote(outbox.at[t], inbox.at[t], send_o.at[t], recv_o.at[t], (me, t)).wait_recv()
        branch = branch + inbox[t].astype(F32)
    out_ref[...] = (x_v[mine].astype(F32) + mods[4:5, :] * branch).astype(BF16)
    for copy in swaps + shipped:
        copy.wait_send()
    sent()


def tables(count, rope):
    quarter = rope // 4
    lane = np.arange(LANES)
    pair = (lane % rope) // 2
    inverse = (np.float32(ROPE_BASE) ** (-(pair % quarter).astype(np.float32) / np.float32(quarter))).astype(np.float32)
    is_row = (pair < quarter)[None, :]
    out = []
    for size, keep in ((count, is_row), (GRID_W, ~is_row)):
        angle = (np.arange(size, dtype=np.float32)[:, None] * inverse[None, :]).astype(np.float32)
        sine = np.sin(angle)
        signed = np.where(lane[None, :] % 2 == 0, -sine, sine)
        out.append(np.stack([np.where(keep, np.cos(angle), 0.0), np.where(keep, signed, 0.0)]).astype(np.float32))
    return out


def body(
    latent, cond, ctx_mod, context, shift_w, scale_w, gate_w, norm_gain, w_qn, w_qr, w_kv_down, w_rope_key,
    kv_gain, w_key_up, w_value_up, ctx_bias, w_out,
):
    n_sp, n_tp = lax.axis_size("sp"), lax.axis_size("tp")
    rows, width = latent.shape
    ctx_rows = context.shape[0]
    tokens = rows * n_tp
    heads = ctx_bias.shape[0]
    nope = w_key_up.shape[1] // heads
    rope = w_rope_key.shape[1]
    rank = w_kv_down.shape[1]
    factor = (nope + rope) ** (-0.5)
    feat, columns = shift_w.shape
    slot_of = Slot(rows, ctx_rows, rank)
    nz = n_sp // 4
    short = -(heads * rope) % LANES
    if short:
        w_qr = jnp.concatenate([w_qr, jnp.zeros((width, short), BF16)], axis=1)
    rowtab, coltab = tables(tokens * n_sp // GRID_W, rope)
    chunk_rows = n_tp * max(2 * rows, 4 * slot_of.ctx * slot_of.planes(n_tp, nz))

    def like(a):
        return pltpu.VMEM(a.shape, a.dtype)

    operands = (
        cond.reshape(n_sp, feat), ctx_mod.reshape(n_sp, feat), shift_w, scale_w, gate_w, latent, context,
        norm_gain[None, :], w_kv_down, w_rope_key.T, kv_gain[None, :], rowtab, coltab, ctx_bias[None, :],
        w_qr, w_qn, w_key_up, w_value_up, w_out,
    )
    staged = [like(a) for a in operands]
    staged[5] = pltpu.VMEM((n_tp, rows, width), BF16)
    dma = pltpu.SemaphoreType.DMA
    return pl.pallas_call(
        functools.partial(kernel, n_sp, n_tp, heads, nope, rope, ctx_rows, factor, slot_of),
        out_shape=jax.ShapeDtypeStruct((rows, width), BF16),
        in_specs=[pl.BlockSpec(memory_space=pl.ANY)] * len(operands),
        out_specs=pl.BlockSpec(memory_space=pltpu.VMEM),
        scratch_shapes=staged + [
            dma((len(operands),)),
            pltpu.VMEM((n_sp, 8, LANES), F32),
            pltpu.VMEM((n_sp, 8, LANES), F32),
            pltpu.VMEM((8, LANES), F32),
            pltpu.VMEM((n_sp * n_tp, 8, LANES), F32),
            pltpu.VMEM((8, width), F32),
            pltpu.VMEM((rows + slot_of.ctx, width), F32),
            pltpu.VMEM((rows + slot_of.ctx, width), BF16),
            pltpu.VMEM((n_tp, rows, width), BF16),
            pltpu.VMEM((tokens, LANES), F32),
            pltpu.VMEM((tokens, LANES), F32),
            pltpu.VMEM((w_value_up.shape[1], rank), BF16),
            pltpu.VMEM((heads, 8, tokens), F32),
            pltpu.VMEM((n_tp, nz, 4, slot_of.height, LANES), BF16),
            pltpu.VMEM((heads, slot_of.split, nope + LANES, tokens), BF16),
            pltpu.VMEM((chunk_rows, heads * nope), BF16),
            pltpu.VMEM((heads * nope, chunk_rows), BF16),
            pltpu.VMEM((heads, nope, tokens), F32),
            pltpu.VMEM((heads, 8, tokens), F32),
            pltpu.VMEM((heads, 8, tokens), F32),
            pltpu.VMEM((tokens, heads * nope), BF16),
            pltpu.VMEM((n_tp, rows, width), BF16),
            pltpu.VMEM((n_tp, rows, width), BF16),
            dma((n_sp,)),
            dma((n_sp,)),
            dma((n_sp * n_tp,)),
            dma((n_sp * n_tp,)),
            dma((n_tp,)),
            dma((n_tp,)),
            dma((4, nz, 4)),
            dma((nz, 4)),
            dma((n_tp, nz, 4)),
            dma((n_tp, nz, 4)),
            dma((n_tp,)),
            dma((n_tp,)),
        ],
        compiler_params=pltpu.CompilerParams(
            collective_id=0, has_side_effects=True, vmem_limit_bytes=62 * 1024 * 1024
        ),
        name="block",
    )(*operands)


def solution(mesh):
    placed = (
        P(("sp", "tp"), None),
        P(),
        P(),
        P(("sp", "tp"), None),
        P("sp", "tp"),
        P("sp", "tp"),
        P("sp", "tp"),
        P(),
        P(None, "tp"),
        P(None, "tp"),
        P(),
        P(),
        P(),
        P(None, "tp"),
        P(None, "tp"),
        P("tp"),
        P("tp", None),
    )
    return jax.shard_map(
        body, mesh=mesh, in_specs=placed, out_specs=P(("sp", "tp"), None), check_vma=False
    )
```

time: 98.2 us -> 86 us (0.88)
  local copies, waits for them, and re-layouts: 9.3 us -> 1.88 us
  other arithmetic: 4.54 us -> 0 us
    unnamed x22 -> x1, local copies, waits for them, and re-layouts: 8.33 us -> 1.88 us
    select_n x4 -> x0, other arithmetic: 1.69 us -> none  [the longest x2 1.66 us: tables(): return (jnp.cos(angle), jnp.where(lane[None, :] % 2 == 0, -sine, sine))]
    mul x2 -> x0, other arithmetic: 1.6 us -> none  [body(): pair = jnp.stack([jax.nn.silu(cond), jax.nn.silu(ctx_mod)])]
    concatenate x1 -> x0, other arithmetic: 1.13 us -> none  [body(): x = jnp.concatenate([latent, context, pad], axis=0)]
    pallas_call x2 -> x1, Pallas kernels: 83.8 us -> 83.3 us  [body(): pl.pallas_call(functools.partial(kernel, n_sp, n_tp, heads, nope, rope, c...]
where the time goes in v1:
time: 86 us; the launch traced here: 85.2 us
  Pallas kernels  83.3 us (97%)
  local copies, waits for them, and re-layouts  1.88 us (2%)
    pallas_call x1, Pallas kernels, body(): pl.pallas_call(functools.partial(kernel, n_sp, n_tp, heads, nope, rope, c...  83.3 us
    unnamed x1, local copies, waits for them, and re-layouts  1.88 us

profile of v1, /device:TPU:1, one launch (start us, length us, event | category | flops | bytes accessed | tf_op | source)
XLA Modules:
  0.0 85.2 jit_solution(6857995795618121427)
XLA Ops:
  0.0 83.3 %block.1 = bf16[128,2048]{1,0:T(8,128)(2,1)} custom-call(f32[16,128]{1,0:T(8,128)} %bitcast.7, f32[16,128]{1,0:T(8,128)} %bitcast.8, f32[128,1024]{1,0:T(8,128)} %shift_hbm.1, f32[128,1024]{1,0:T(8,128)} %scale_hbm.1, f32[128,1024]{1,0:T(8,128)} %gate_hbm.1, bf16[128,2048]{1,0:T(8,128)(2,1)} %latent_hbm.1, bf16[16,2048]{1,0:T(8,128)(2,1)} %context_hbm.1, ...), custom_call_target="tpu_custom_call" | custom-call | tf_op jit(solution)/shard_map/block/pallas_call | solution.py:529
  83.3 1.9 %copy.21 = bf16[128,2048]{1,0:T(8,128)(2,1)} copy(bf16[128,2048]{1,0:T(8,128)(2,1)} %block.1) | data formatting | bytes 1048576

commit v2 on v1

--- a/solution.py
+++ b/solution.py
@@ -65,7 +65,7 @@
     cond_v, ctxm_v, shift_v, scale_v, gate_v, x_v, ctx_v, gain_v, down_v, rope_v, kvg_v, rowtab_v, coltab_v, bias_v,
     qr_v, qn_v, ku_v, vu_v, wo_v, load_sem,
     part, landed, reduced, full, mods, normed, hown, hfull, cos_v, sin_v, vut, bias_b,
-    buf, qt, kbuf, vt, acc, top, total_v, att, outbox, inbox,
+    buf, qt, kbuf, vt, sbuf, acc, top, total_v, att, outbox, inbox,
     send1, recv1, send2, recv2, send_x, recv_x, send, recv, send_t, recv_t, send_o, recv_o,
 ):
     me = lax.axis_index("sp")
@@ -357,31 +357,51 @@
 
     def process(lat, ropes, biased=False, valid=None):
         count = lat.shape[0]
-        piece_rows = count // len(ropes)
-        for at in range(0, heads * nope, wide):
+        tall = count // len(ropes)
+        share = wide // nope
+
+        def raise_keys(at):
             kbuf[:count, at : at + wide] = dot(lat, ku_v[:, at : at + wide]).astype(BF16)
+
+        def raise_values(at):
             vt[at : at + wide, :count] = dot_nt(vut[at : at + wide, :], lat).astype(BF16)
-        for head in range(heads):
-            pieces = []
-            for g, rope_rows in enumerate(ropes):
+
+        def score(head):
+            if head % share == 0:
+                raise_keys(head * nope)
+            high = None
+            for g, shared in enumerate(ropes):
                 keys = jnp.concatenate(
-                    [kbuf[g * piece_rows : (g + 1) * piece_rows, head * nope : (head + 1) * nope], rope_rows], axis=1
+                    [kbuf[g * tall : (g + 1) * tall, head * nope : (head + 1) * nope], shared], axis=1
                 )
-                pieces.append(dot(keys, qt[head, g]))
-            scores = jnp.concatenate(pieces, axis=0)
-            if valid is not None:
-                scores = jnp.where(valid, scores, -1e30)
+                piece = dot(keys, qt[head, g])
+                if valid is not None:
+                    piece = jnp.where(valid, piece, -1e30)
+                sbuf[head % 2, g * tall : (g + 1) * tall] = piece
+                peak = jnp.max(piece, axis=0, keepdims=True)
+                high = peak if high is None else jnp.maximum(high, peak)
+            return high
+
+        def soften(head, high):
             old = top[head][:1]
-            high = jnp.max(scores, axis=0, keepdims=True)
             if biased:
                 high = high + bias_b[head][:1]
             new = jnp.maximum(old, high)
             less = new - bias_b[head][:1] if biased else new
-            weights = jnp.exp2(scores - less)
+            weights = jnp.exp2(sbuf[head % 2, :count] - less)
             fade = jnp.exp2(old - new)
             top[head] = jnp.broadcast_to(new, top.shape[1:])
             total_v[head] = total_v[head] * fade + jnp.sum(weights, axis=0, keepdims=True)
             acc[head] = acc[head] * fade + dot(vt[head * nope : (head + 1) * nope, :count], weights.astype(BF16))
+
+        high = score(0)
+        raise_values(0)
+        for head in range(heads):
+            later = score(head + 1) if head + 1 < heads else None
+            if head + 1 < heads and (head + 1) % share == 0:
+                raise_values((head + 1) * nope)
+            soften(head, high)
+            high = later
 
     def chunk(k):
         step, half = k // 2, k % 2
@@ -549,6 +569,7 @@
             pltpu.VMEM((heads, slot_of.split, nope + LANES, tokens), BF16),
             pltpu.VMEM((chunk_rows, heads * nope), BF16),
             pltpu.VMEM((heads * nope, chunk_rows), BF16),
+            pltpu.VMEM((2, chunk_rows, tokens), F32),
             pltpu.VMEM((heads, nope, tokens), F32),
             pltpu.VMEM((heads, 8, tokens), F32),
             pltpu.VMEM((heads, 8, tokens), F32),

time: 86 us -> 77.9 us (0.906)
  Pallas kernels: 83.3 us -> 75.2 us
    pallas_call x1, Pallas kernels: 83.3 us -> 75.2 us  [body(): pl.pallas_call(functools.partial(kernel, n_sp, n_tp, heads, nope, rope, c...]
where the time goes in v2:
time: 77.9 us; the launch traced here: 77.1 us
  Pallas kernels  75.2 us (97%)
  local copies, waits for them, and re-layouts  1.88 us (2%)
    pallas_call x1, Pallas kernels, body(): pl.pallas_call(functools.partial(kernel, n_sp, n_tp, heads, nope, rope, c...  75.2 us
    unnamed x1, local copies, waits for them, and re-layouts  1.88 us

profile of v2, /device:TPU:1, one launch (start us, length us, event | category | flops | bytes accessed | tf_op | source)
XLA Modules:
  0.0 77.1 jit_solution(12262484381635302583)
XLA Ops:
  0.0 75.2 %block.1 = bf16[128,2048]{1,0:T(8,128)(2,1)} custom-call(f32[16,128]{1,0:T(8,128)} %bitcast.7, f32[16,128]{1,0:T(8,128)} %bitcast.8, f32[128,1024]{1,0:T(8,128)} %shift_hbm.1, f32[128,1024]{1,0:T(8,128)} %scale_hbm.1, f32[128,1024]{1,0:T(8,128)} %gate_hbm.1, bf16[128,2048]{1,0:T(8,128)(2,1)} %latent_hbm.1, bf16[16,2048]{1,0:T(8,128)(2,1)} %context_hbm.1, ...), custom_call_target="tpu_custom_call" | custom-call | tf_op jit(solution)/shard_map/block/pallas_call | solution.py:549
  75.2 1.9 %copy.21 = bf16[128,2048]{1,0:T(8,128)(2,1)} copy(bf16[128,2048]{1,0:T(8,128)(2,1)} %block.1) | data formatting | bytes 1048576

commit v3 on v2

--- a/solution.py
+++ b/solution.py
@@ -14,6 +14,11 @@
 LANES = 128
 LOG2E = 1.4426950408889634
 MODS = 5
+ORDERS = {
+    4: (
+        ("a0", "z1", "b0", "z2"), ("d0", "a1", "z3", "b1"), ("a2", "b2"), ("d1",), ("d2", "a3"), ("b3",), ("d3",), (),
+    )
+}
 MESH = pl.DeviceIdType.MESH
 F32 = jnp.float32
 BF16 = jnp.bfloat16
@@ -64,14 +69,12 @@
     out_ref,
     cond_v, ctxm_v, shift_v, scale_v, gate_v, x_v, ctx_v, gain_v, down_v, rope_v, kvg_v, rowtab_v, coltab_v, bias_v,
     qr_v, qn_v, ku_v, vu_v, wo_v, load_sem,
-    part, landed, reduced, full, mods, normed, hown, hfull, cos_v, sin_v, vut, bias_b,
+    part, land1, sum1, land2, sum2, land3, mods, normed, hown, hfull, cos_v, sin_v, vut, bias_b,
     buf, qt, kbuf, vt, sbuf, acc, top, total_v, att, outbox, inbox,
-    send1, recv1, send2, recv2, send_x, recv_x, send, recv, send_t, recv_t, send_o, recv_o,
+    send1, recv1, send2, recv2, send3, recv3, send_x, recv_x, send, recv, send_t, recv_t, send_o, recv_o,
 ):
     me = lax.axis_index("sp")
     mine = lax.axis_index("tp")
-    total = n_sp * n_tp
-    flat = me * n_tp + mine
     barrier = pltpu.get_barrier_semaphore()
     rows, rank = slot_of.rows, ku_v.shape[0]
     depth = x_v.shape[2]
@@ -93,19 +96,18 @@
         if name not in late:
             loads[name].start()
 
-    part[...] = jnp.zeros_like(part)
-    landed[...] = jnp.zeros_like(landed)
-
-    def greet(i, _):
-        other = lax.rem(flat + i, total)
-        pl.semaphore_signal(barrier, inc=1, device_id=(other // n_tp, other % n_tp), device_id_type=MESH)
-        return 0
-
-    lax.fori_loop(1, total, greet, 0)
+    nz = n_sp // 4
+    z, side = me // 4, me % 4
+    others = [lax.rem(side + i, 4) for i in range(1, 4)]
+    levels = [lax.rem(z + i, nz) for i in range(1, nz)]
+    greeted = [(z * 4 + s, mine) for s in others] + [(k * 4 + side, mine) for k in levels] + [(me, t) for t in partners]
+    for other in greeted:
+        pl.semaphore_signal(barrier, inc=1, device_id=other, device_id_type=MESH)
 
     feat, columns = shift_v.shape
     blocks = columns // LANES
-    per = -(-MODS * blocks // n_sp)
+    if part.shape[0] != MODS * blocks:
+        part[...] = jnp.zeros_like(part)
     sides = []
     for name, ref in (("cond", cond_v), ("ctxm", ctxm_v)):
         loads[name].wait()
@@ -118,28 +120,35 @@
             loads[name].wait()
         for block in range(blocks):
             unit = row * blocks + block
-            part[unit // per, unit % per : unit % per + 1, :] = jnp.sum(
+            part[unit : unit + 1, :] = jnp.sum(
                 weight[:, block * LANES : (block + 1) * LANES] * sides[which], axis=0, keepdims=True
             )
     for name in late:
         loads[name].start()
-    pl.semaphore_wait(barrier, total - 1)
-
-    some = pl.ds(0, per)
-
-    def scattering(other):
-        return remote(part.at[other, some], landed.at[me, some], send1.at[other], recv1.at[me], (other, mine))
-
-    def scatter(i, _):
-        scattering(lax.rem(me + i, n_sp)).start()
-        return 0
-
-    lax.fori_loop(1, n_sp, scatter, 0)
+    pl.semaphore_wait(barrier, len(greeted))
+
+    def spread(src, dst, at, sends, recvs, devices):
+        copies = [
+            remote(src, dst.at[at], sends.at[i], recvs.at[at], device) for i, device in enumerate(devices)
+        ]
+        for copy in copies:
+            copy.start()
+        return copies
+
+    def fold(dst, recvs, indices):
+        for i in indices:
+            remote(dst.at[i], dst.at[i], send1.at[0], recvs.at[i], greeted[0]).wait_recv()
+        total = dst[0]
+        for i in range(1, dst.shape[0]):
+            total = total + dst[i]
+        return total
+
+    sends = spread(part, land1, side, send1, recv1, [(z * 4 + s, mine) for s in others])
+    land1[side] = part[...]
     loads["x"].wait()
     swaps = [remote(x_v.at[mine], x_v.at[mine], send_x.at[t], recv_x.at[mine], (me, t)) for t in partners]
     for swap in swaps:
         swap.start()
-    landed[me] = part[me]
 
     loads["gain"].wait()
     loads["ctx"].wait()
@@ -164,23 +173,9 @@
         cos_v[at] = coltab_v[0] + rowtab_v[0, line]
         sin_v[at] = coltab_v[1] + rowtab_v[1, line]
 
-    def scattered(i, _):
-        other = lax.rem(me + i, n_sp)
-        remote(part.at[other, some], landed.at[other, some], send1.at[other], recv1.at[other], (other, mine)).wait()
-        return 0
-
-    lax.fori_loop(1, n_sp, scattered, 0)
-    reduced[...] = jnp.sum(landed[...], axis=0)
-
-    def gather(i, _):
-        other = lax.rem(flat + i, total)
-        remote(
-            reduced.at[some], full.at[flat, some], send2.at[other], recv2.at[flat], (other // n_tp, other % n_tp)
-        ).start()
-        return 0
-
-    lax.fori_loop(1, total, gather, 0)
-    full[flat] = reduced[...]
+    sum1[...] = fold(land1, recv1, others)
+    sends += spread(sum1, land2, z, send2, recv2, [(k * 4 + side, mine) for k in levels])
+    land2[z] = sum1[...]
 
     loads["vu"].wait()
     for at in range(0, vu_v.shape[1], LANES):
@@ -191,23 +186,19 @@
     acc[...] = jnp.zeros_like(acc)
     top[...] = jnp.full(top.shape, -1e30, F32)
     total_v[...] = jnp.zeros_like(total_v)
+    sum2[...] = fold(land2, recv2, levels)
+    sends += spread(sum2, land3, mine, send3, recv3, [(me, t) for t in partners])
+    land3[mine] = sum2[...]
     loads["down"].wait()
     loads["rope"].wait()
     loads["kvg"].wait()
-
-    def gathered(i, _):
-        other = lax.rem(flat + i, total)
-        remote(
-            reduced.at[some], full.at[other, some], send2.at[other], recv2.at[other], (other // n_tp, other % n_tp)
-        ).wait()
-        return 0
-
-    lax.fori_loop(1, total, gathered, 0)
+    for t in partners:
+        remote(land3.at[t], land3.at[t], send1.at[0], recv3.at[t], greeted[0]).wait_recv()
     for unit in range(MODS * blocks):
         row, block = unit // blocks, unit % blocks
         for t in range(n_tp):
             at = t * columns + block * LANES
-            mods[row : row + 1, at : at + LANES] = full[(unit // per) * n_tp + t, unit % per : unit % per + 1, :]
+            mods[row : row + 1, at : at + LANES] = land3[t, unit : unit + 1, :]
 
     def modulate(values, which):
         return (values * (1.0 + mods[2 + which : 3 + which, :]) + mods[which : which + 1, :]).astype(BF16)
@@ -223,8 +214,6 @@
     own_rows = pl.ds(pl.multiple_of(mine * rows, rows), rows)
     turned = rotate(key[:rows], cos_v[own_rows], sin_v[own_rows])
 
-    nz = n_sp // 4
-    z, side = me // 4, me % 4
     y, x = side // 2, side % 2
     odd = mine % 2
     flip_x = y * 2 + (1 - x)
@@ -432,12 +421,16 @@
         )
         process(lat, [ropes] * slot_of.split)
 
+    kinds = {"z": event_z, "a": event_a, "b": lambda p: event_b(p, side_b), "d": lambda p: event_b(p, side_ab)}
+    agenda = ORDERS.get(nz)
+    if agenda is None:
+        agenda = [
+            [f"a{k}"] * (k < nz) + [f"z{k + 1}"] * (k + 1 < nz) + [f"{'bd'[k % 2]}{k // 2}"] for k in range(2 * nz)
+        ]
+
     def before(k):
-        if k < nz:
-            event_a(k)
-        if k + 1 < nz:
-            event_z(k + 1)
-        event_b(k // 2, side_b if k % 2 == 0 else side_ab)
+        for name in agenda[k]:
+            kinds[name[0]](int(name[1:]))
 
     def turn(k, _):
         for i in range(2 * nz):
@@ -493,7 +486,7 @@
         remote(outbox.at[t], inbox.at[t], send_o.at[t], recv_o.at[t], (me, t)).wait_recv()
         branch = branch + inbox[t].astype(F32)
     out_ref[...] = (x_v[mine].astype(F32) + mods[4:5, :] * branch).astype(BF16)
-    for copy in swaps + shipped:
+    for copy in sends + swaps + shipped:
         copy.wait_send()
     sent()
 
@@ -529,6 +522,7 @@
     feat, columns = shift_w.shape
     slot_of = Slot(rows, ctx_rows, rank)
     nz = n_sp // 4
+    units = -(-MODS * (columns // LANES) // 8) * 8
     short = -(heads * rope) % LANES
     if short:
         w_qr = jnp.concatenate([w_qr, jnp.zeros((width, short), BF16)], axis=1)
@@ -553,10 +547,12 @@
         out_specs=pl.BlockSpec(memory_space=pltpu.VMEM),
         scratch_shapes=staged + [
             dma((len(operands),)),
-            pltpu.VMEM((n_sp, 8, LANES), F32),
-            pltpu.VMEM((n_sp, 8, LANES), F32),
-            pltpu.VMEM((8, LANES), F32),
-            pltpu.VMEM((n_sp * n_tp, 8, LANES), F32),
+            pltpu.VMEM((units, LANES), F32),
+            pltpu.VMEM((4, units, LANES), F32),
+            pltpu.VMEM((units, LANES), F32),
+            pltpu.VMEM((nz, units, LANES), F32),
+            pltpu.VMEM((units, LANES), F32),
+            pltpu.VMEM((n_tp, units, LANES), F32),
             pltpu.VMEM((8, width), F32),
             pltpu.VMEM((rows + slot_of.ctx, width), F32),
             pltpu.VMEM((rows + slot_of.ctx, width), BF16),
@@ -576,10 +572,12 @@
             pltpu.VMEM((tokens, heads * nope), BF16),
             pltpu.VMEM((n_tp, rows, width), BF16),
             pltpu.VMEM((n_tp, rows, width), BF16),
-            dma((n_sp,)),
-            dma((n_sp,)),
-            dma((n_sp * n_tp,)),
-            dma((n_sp * n_tp,)),
+            dma((4,)),
+            dma((4,)),
+            dma((nz,)),
+            dma((nz,)),
+            dma((n_tp,)),
+            dma((n_tp,)),
             dma((n_tp,)),
             dma((n_tp,)),
             dma((4, nz, 4)),

time: 77.9 us -> 64.2 us (0.82)
  Pallas kernels: 75.2 us -> 61.5 us
    pallas_call x1, Pallas kernels: 75.2 us -> 61.5 us  [body(): pl.pallas_call(functools.partial(kernel, n_sp, n_tp, heads, nope, rope, c...]
where the time goes in v3:
time: 64.2 us; the launch traced here: 63.4 us
  Pallas kernels  61.5 us (96%)
  local copies, waits for them, and re-layouts  1.88 us (3%)
    pallas_call x1, Pallas kernels, body(): pl.pallas_call(functools.partial(kernel, n_sp, n_tp, heads, nope, rope, c...  61.5 us
    unnamed x1, local copies, waits for them, and re-layouts  1.88 us

profile of v3, /device:TPU:1, one launch (start us, length us, event | category | flops | bytes accessed | tf_op | source)
XLA Modules:
  0.0 63.4 jit_solution(13088189409075974480)
XLA Ops:
  0.0 61.5 %block.1 = bf16[128,2048]{1,0:T(8,128)(2,1)} custom-call(f32[16,128]{1,0:T(8,128)} %bitcast.7, f32[16,128]{1,0:T(8,128)} %bitcast.8, f32[128,1024]{1,0:T(8,128)} %shift_hbm.1, f32[128,1024]{1,0:T(8,128)} %scale_hbm.1, f32[128,1024]{1,0:T(8,128)} %gate_hbm.1, bf16[128,2048]{1,0:T(8,128)(2,1)} %latent_hbm.1, bf16[16,2048]{1,0:T(8,128)(2,1)} %context_hbm.1, ...), custom_call_target="tpu_custom_call" | custom-call | tf_op jit(solution)/shard_map/block/pallas_call | solution.py:543
  61.5 1.9 %copy.21 = bf16[128,2048]{1,0:T(8,128)(2,1)} copy(bf16[128,2048]{1,0:T(8,128)(2,1)} %block.1) | data formatting | bytes 1048576

commit v4 on v3

--- a/solution.py
+++ b/solution.py
@@ -16,7 +16,7 @@
 MODS = 5
 ORDERS = {
     4: (
-        ("a0", "z1", "b0", "z2"), ("d0", "a1", "z3", "b1"), ("a2", "b2"), ("d1",), ("d2", "a3"), ("b3",), ("d3",), (),
+        ("a0", "z1", "b0", "z2"), ("d0", "a1"), ("a2", "b1", "z3", "d1"), ("b2", "d2"), ("a3",), ("b3",), ("d3",), (),
     )
 }
 MESH = pl.DeviceIdType.MESH
@@ -52,10 +52,10 @@
         self.rows = rows
         self.ctx = -(-ctx_rows // 16) * 16
         self.columns = rank // LANES
-        self.rope_at = self.columns * rows
+        self.stride = rows + self.ctx
+        self.rope_at = self.columns * self.stride
         self.rope_rows = rows // self.split
-        self.ctx_at = self.rope_at + self.rope_rows
-        self.ctx_rope_at = self.ctx_at + self.columns * self.ctx
+        self.ctx_rope_at = self.rope_at + self.rope_rows
         self.height = self.ctx_rope_at + self.ctx
 
     def planes(self, n_tp, nz):
@@ -69,8 +69,8 @@
     out_ref,
     cond_v, ctxm_v, shift_v, scale_v, gate_v, x_v, ctx_v, gain_v, down_v, rope_v, kvg_v, rowtab_v, coltab_v, bias_v,
     qr_v, qn_v, ku_v, vu_v, wo_v, load_sem,
-    part, land1, sum1, land2, sum2, land3, mods, normed, hown, hfull, cos_v, sin_v, vut, bias_b,
-    buf, qt, kbuf, vt, sbuf, acc, top, total_v, att, outbox, inbox,
+    part, land1, sum1, land2, sum2, land3, mods, normed, hown, hfull, cos_v, sin_v, vut, kut, bias_b,
+    buf, qt, dense, kbuf, vt, sbuf, acc, top, total_v, att, outbox, inbox,
     send1, recv1, send2, recv2, send3, recv3, send_x, recv_x, send, recv, send_t, recv_t, send_o, recv_o,
 ):
     me = lax.axis_index("sp")
@@ -225,13 +225,13 @@
     own = (mine, z, side)
     for c in range(slot_of.columns):
         lanes = slice(c * LANES, (c + 1) * LANES)
-        buf[mine, z, side, c * rows : (c + 1) * rows] = inner[:rows, lanes]
-        at = slot_of.ctx_at + c * ctx
+        buf[mine, z, side, c * slot_of.stride : c * slot_of.stride + rows] = inner[:rows, lanes]
+        at = c * slot_of.stride + rows
         buf[mine, z, side, at : at + ctx] = inner[rows:, lanes]
     shared = turned[: slot_of.rope_rows]
     if slot_of.split == 2:
         shared = shared + pltpu.roll(turned[slot_of.rope_rows :], rope, 1)
-    buf[mine, z, side, slot_of.rope_at : slot_of.ctx_at] = shared.astype(BF16)
+    buf[mine, z, side, slot_of.rope_at : slot_of.ctx_rope_at] = shared.astype(BF16)
     buf[mine, z, side, slot_of.ctx_rope_at :] = key[rows:].astype(BF16)
 
     def plane(step, t):
@@ -343,17 +343,20 @@
             for g in range(slot_of.split):
                 qt[at // nope + k, g, :nope, :] = value
     loads["ku"].wait()
+    for at in range(0, ku_v.shape[1], LANES):
+        kut[at : at + LANES, :] = ku_v[:, at : at + LANES].T
 
     def process(lat, ropes, biased=False, valid=None):
         count = lat.shape[0]
+        dense[:count] = lat
         tall = count // len(ropes)
         share = wide // nope
 
         def raise_keys(at):
-            kbuf[:count, at : at + wide] = dot(lat, ku_v[:, at : at + wide]).astype(BF16)
+            kbuf[:count, at : at + wide] = dot_nt(dense[:count], kut[at : at + wide, :]).astype(BF16)
 
         def raise_values(at):
-            vt[at : at + wide, :count] = dot_nt(vut[at : at + wide, :], lat).astype(BF16)
+            vt[at : at + wide, :count] = dot_nt(vut[at : at + wide, :], dense[:count]).astype(BF16)
 
         def score(head):
             if head % share == 0:
@@ -384,30 +387,25 @@
             acc[head] = acc[head] * fade + dot(vt[head * nope : (head + 1) * nope, :count], weights.astype(BF16))
 
         high = score(0)
-        raise_values(0)
         for head in range(heads):
             later = score(head + 1) if head + 1 < heads else None
-            if head + 1 < heads and (head + 1) % share == 0:
-                raise_values((head + 1) * nope)
+            if head % share == 0:
+                raise_values(head * nope)
             soften(head, high)
             high = later
 
-    def chunk(k):
-        step, half = k // 2, k % 2
-        pair = (
-            jnp.where(half == 0, side, flip_y),
-            jnp.where(half == 0, flip_x, side_ab),
-        )
-        places = [(t, plane(step, t), ss) for t in range(n_tp) for ss in pair]
+    def chunk(entries):
+        places = [(t, plane(step, t), ss) for t in range(n_tp) for step, ss in entries]
         for t in partners:
-            zz = plane(step, t)
-            for ss in pair:
+            for step, ss in entries:
+                zz = plane(step, t)
                 remote(slot(t, zz, ss), slot(t, zz, ss), send_t.at[t, zz, ss], recv_t.at[t, zz, ss], (me, t)).wait_recv()
         tall = slot_of.rope_rows
 
         def block(place, c, g):
             t, zz, ss = place
-            return buf[t, zz, ss, c * rows + g * tall : c * rows + (g + 1) * tall]
+            at = c * slot_of.stride + g * tall
+            return buf[t, zz, ss, at : at + tall]
 
         lat = jnp.concatenate(
             [
@@ -417,7 +415,7 @@
             axis=1,
         )
         ropes = jnp.concatenate(
-            [buf[t, zz, ss, slot_of.rope_at : slot_of.ctx_at] for t, zz, ss in places], axis=0
+            [buf[t, zz, ss, slot_of.rope_at : slot_of.ctx_rope_at] for t, zz, ss in places], axis=0
         )
         process(lat, [ropes] * slot_of.split)
 
@@ -433,12 +431,21 @@
             kinds[name[0]](int(name[1:]))
 
     def turn(k, _):
-        for i in range(2 * nz):
+        for i in range(2 * nz - 1):
             pl.when(k == i)(functools.partial(before, i))
-        chunk(k)
+        step, late = k // 2, k % 2
+        chunk(
+            [
+                (step, flip_x * (1 - late) + side_ab * late),
+                (step + late, flip_y * (1 - late) + side * late),
+            ]
+        )
         return 0
 
-    lax.fori_loop(0, 2 * nz, turn, 0)
+    chunk([(0, side)])
+    lax.fori_loop(0, 2 * nz - 1, turn, 0)
+    before(2 * nz - 1)
+    chunk([(nz - 1, side_ab)])
 
     per_plane = slot_of.planes(n_tp, nz)
 
@@ -450,7 +457,7 @@
             [
                 jnp.concatenate(
                     [
-                        buf[t, zz, ss, slot_of.ctx_at + c * ctx : slot_of.ctx_at + (c + 1) * ctx]
+                        buf[t, zz, ss, c * slot_of.stride + rows : (c + 1) * slot_of.stride]
                         for t, zz, ss in places
                     ],
                     axis=0,
@@ -560,9 +567,11 @@
             pltpu.VMEM((tokens, LANES), F32),
             pltpu.VMEM((tokens, LANES), F32),
             pltpu.VMEM((w_value_up.shape[1], rank), BF16),
+            pltpu.VMEM((w_key_up.shape[1], rank), BF16),
             pltpu.VMEM((heads, 8, tokens), F32),
             pltpu.VMEM((n_tp, nz, 4, slot_of.height, LANES), BF16),
             pltpu.VMEM((heads, slot_of.split, nope + LANES, tokens), BF16),
+            pltpu.VMEM((chunk_rows, rank), BF16),
             pltpu.VMEM((chunk_rows, heads * nope), BF16),
             pltpu.VMEM((heads * nope, chunk_rows), BF16),
             pltpu.VMEM((2, chunk_rows, tokens), F32),

time: 64.2 us -> 62.1 us (0.967)
  Pallas kernels: 61.5 us -> 60 us
    pallas_call x1, Pallas kernels: 61.5 us -> 60 us  [body(): pl.pallas_call(functools.partial(kernel, n_sp, n_tp, heads, nope, rope, c...]
where the time goes in v4:
time: 62.1 us; the launch traced here: 61.9 us
  Pallas kernels  60 us (97%)
  local copies, waits for them, and re-layouts  1.88 us (3%)
    pallas_call x1, Pallas kernels, body(): pl.pallas_call(functools.partial(kernel, n_sp, n_tp, heads, nope, rope, c...  60 us
    unnamed x1, local copies, waits for them, and re-layouts  1.88 us

profile of v4, /device:TPU:1, one launch (start us, length us, event | category | flops | bytes accessed | tf_op | source)
XLA Modules:
  0.0 61.9 jit_solution(12824759024955176327)
XLA Ops:
  0.0 60.0 %block.1 = bf16[128,2048]{1,0:T(8,128)(2,1)} custom-call(f32[16,128]{1,0:T(8,128)} %bitcast.7, f32[16,128]{1,0:T(8,128)} %bitcast.8, f32[128,1024]{1,0:T(8,128)} %shift_hbm.1, f32[128,1024]{1,0:T(8,128)} %scale_hbm.1, f32[128,1024]{1,0:T(8,128)} %gate_hbm.1, bf16[128,2048]{1,0:T(8,128)(2,1)} %latent_hbm.1, bf16[16,2048]{1,0:T(8,128)(2,1)} %context_hbm.1, ...), custom_call_target="tpu_custom_call" | custom-call | tf_op jit(solution)/shard_map/block/pallas_call | solution.py:550
  60.0 1.9 %copy.21 = bf16[128,2048]{1,0:T(8,128)(2,1)} copy(bf16[128,2048]{1,0:T(8,128)(2,1)} %block.1) | data formatting | bytes 1048576

commit v5 on v4

--- a/solution.py
+++ b/solution.py
@@ -484,15 +484,24 @@
     shipped = []
     for t in partners:
         lines = pl.ds(pl.multiple_of(t * rows, rows), rows)
-        outbox[t] = dot(att[lines, :], wo_v[...]).astype(BF16)
-        copy = remote(outbox.at[t], inbox.at[mine], send_o.at[t], recv_o.at[mine], (me, t))
-        copy.start()
-        shipped.append(copy)
+        for part_of in range(2):
+            cut = slice(part_of * depth // 2, (part_of + 1) * depth // 2)
+            outbox[part_of, t] = dot(att[lines, :], wo_v[:, cut]).astype(BF16)
+            copy = remote(
+                outbox.at[part_of, t], inbox.at[part_of, mine], send_o.at[part_of, t], recv_o.at[part_of, mine], (me, t)
+            )
+            copy.start()
+            shipped.append(copy)
     branch = dot(att[own_rows, :], wo_v[...]).astype(BF16).astype(F32)
-    for t in partners:
-        remote(outbox.at[t], inbox.at[t], send_o.at[t], recv_o.at[t], (me, t)).wait_recv()
-        branch = branch + inbox[t].astype(F32)
-    out_ref[...] = (x_v[mine].astype(F32) + mods[4:5, :] * branch).astype(BF16)
+    for part_of in range(2):
+        cut = slice(part_of * depth // 2, (part_of + 1) * depth // 2)
+        piece = branch[:, cut]
+        for t in partners:
+            remote(
+                outbox.at[part_of, t], inbox.at[part_of, t], send_o.at[part_of, t], recv_o.at[part_of, t], (me, t)
+            ).wait_recv()
+            piece = piece + inbox[part_of, t].astype(F32)
+        out_ref[:, cut] = (x_v[mine, :, cut].astype(F32) + mods[4:5, cut] * piece).astype(BF16)
     for copy in sends + swaps + shipped:
         copy.wait_send()
     sent()
@@ -579,8 +588,8 @@
             pltpu.VMEM((heads, 8, tokens), F32),
             pltpu.VMEM((heads, 8, tokens), F32),
             pltpu.VMEM((tokens, heads * nope), BF16),
-            pltpu.VMEM((n_tp, rows, width), BF16),
-            pltpu.VMEM((n_tp, rows, width), BF16),
+            pltpu.VMEM((2, n_tp, rows, width // 2), BF16),
+            pltpu.VMEM((2, n_tp, rows, width // 2), BF16),
             dma((4,)),
             dma((4,)),
             dma((nz,)),
@@ -593,8 +602,8 @@
             dma((nz, 4)),
             dma((n_tp, nz, 4)),
             dma((n_tp, nz, 4)),
-            dma((n_tp,)),
-            dma((n_tp,)),
+            dma((2, n_tp)),
+            dma((2, n_tp)),
         ],
         compiler_params=pltpu.CompilerParams(
             collective_id=0, has_side_effects=True, vmem_limit_bytes=62 * 1024 * 1024

time: 62.1 us -> 61.8 us (level)
  no operation moved by 1% of the time
where the time goes in v5:
time: 61.8 us; the launch traced here: 61.6 us
  Pallas kernels  59.7 us (97%)
  local copies, waits for them, and re-layouts  1.88 us (3%)
    pallas_call x1, Pallas kernels, body(): pl.pallas_call(functools.partial(kernel, n_sp, n_tp, heads, nope, rope, c...  59.7 us
    unnamed x1, local copies, waits for them, and re-layouts  1.88 us

profile of v5, /device:TPU:1, one launch (start us, length us, event | category | flops | bytes accessed | tf_op | source)
XLA Modules:
  0.0 61.6 jit_solution(15094690148190396708)
XLA Ops:
  0.0 59.7 %block.1 = bf16[128,2048]{1,0:T(8,128)(2,1)} custom-call(f32[16,128]{1,0:T(8,128)} %bitcast.7, f32[16,128]{1,0:T(8,128)} %bitcast.8, f32[128,1024]{1,0:T(8,128)} %shift_hbm.1, f32[128,1024]{1,0:T(8,128)} %scale_hbm.1, f32[128,1024]{1,0:T(8,128)} %gate_hbm.1, bf16[128,2048]{1,0:T(8,128)(2,1)} %latent_hbm.1, bf16[16,2048]{1,0:T(8,128)(2,1)} %context_hbm.1, ...), custom_call_target="tpu_custom_call" | custom-call | tf_op jit(solution)/shard_map/block/pallas_call | solution.py:559
  59.7 1.9 %copy.21 = bf16[128,2048]{1,0:T(8,128)(2,1)} copy(bf16[128,2048]{1,0:T(8,128)(2,1)} %block.1) | data formatting | bytes 1048576
